TPU v7x, 32 devices: a whole 2x2x4 slice. The times are simulated.
32 devices in a mesh: rep: 2 (over x), fs: 4 (over z), tp: 4 (over y, core).
Axes of the slice: x: 2, y: 2, z: 4, core: 2. Of those that a mesh axis runs over, the one named last changes fastest.
Arguments:
- tokens: bfloat16 [8, 1024, 2048], P(('rep', 'fs')), may hold values from -6 to 6
- mix_gain: bfloat16 [2048], replicated, may hold values from 0.099609375 to 1.8984375
- value_weight: bfloat16 [2048, 1024], P('fs', 'tp'), may hold values from -0.125 to 0.125
- gate_weight: bfloat16 [2048, 1024], P('fs', 'tp'), may hold values from -0.125 to 0.125
- mix_taps: bfloat16 [31, 1024], P(None, 'tp'), may hold values from -1 to 1
- head_gain: bfloat16 [1024], P('tp'), may hold values from 0.099609375 to 1.8984375
- out_weight: bfloat16 [1024, 2048], P('fs', 'tp'), may hold values from -0.1875 to 0.1875
- ffn_gain: bfloat16 [2048], replicated, may hold values from 0.099609375 to 1.8984375
- ffgate_weight: bfloat16 [2048, 6144], P('fs', 'tp'), may hold values from -0.125 to 0.125
- up_weight: bfloat16 [2048, 6144], P('fs', 'tp'), may hold values from -0.125 to 0.125
- ff_taps: bfloat16 [3, 6144], P(None, 'tp'), may hold values from -3.5 to 3.5
- down_weight: bfloat16 [2048, 6144], P('fs', 'tp'), may hold values from -0.078125 to 0.078125
Outputs:
- layer_out: bfloat16 [8, 1024, 2048], P(('rep', 'fs'), 'tp')
All inputs are finite; a program needn't handle non-finite values.
Results may differ from a plain program's by a relative error of at most 0.01.
Values may be sent and summed in bfloat16 or wider, within the bound.
A program may use at most 128 MiB of HBM per device.

v0:
```python
import jax
import jax.numpy as jnp
from jax import lax
from jax.sharding import PartitionSpec as P

HEAD = 128


norm_floor = 0.01


def row_norm(floats_in, scales):
    floats = floats_in.astype(jnp.float32)
    scaled = floats * lax.rsqrt(jnp.mean(floats * floats, axis=-1, keepdims=True) + norm_floor)
    return (scaled * scales.astype(jnp.float32)).astype(jnp.bfloat16)


def causal_conv(signal, kernel_taps):
    reach = kernel_taps.shape[0]
    length = signal.shape[0]
    padded = jnp.pad(signal, ((reach - 1, 0), (0, 0)))
    summed = padded[0:length] * kernel_taps[0]
    for offset in range(1, reach):
        summed = summed + padded[offset : offset + length] * kernel_taps[offset]
    return summed


def head_norm(signal, scales):
    length = signal.shape[0]
    grouped = signal.reshape(length, signal.shape[1] // HEAD, HEAD)
    centre = grouped - jnp.mean(grouped, axis=-1, keepdims=True)
    spread = jnp.mean(centre * centre, axis=-1, keepdims=True)
    normal = (centre * lax.rsqrt(spread + norm_floor)).reshape(signal.shape)
    return normal * scales.astype(jnp.float32)


def on_device(
    tokens,
    mix_gain,
    value_weight,
    gate_weight,
    mix_taps,
    head_gain,
    out_weight,
    ffn_gain,
    ffgate_weight,
    up_weight,
    ff_taps,
    down_weight,
):
    sequence = tokens[0]
    value_full, gate_full, out_full = (
        lax.all_gather(value_weight, "fs", axis=0, tiled=True),
        lax.all_gather(gate_weight, "fs", axis=0, tiled=True),
        lax.all_gather(out_weight, "fs", axis=0, tiled=True),
    )
    normed = row_norm(sequence, mix_gain)
    values = jnp.dot(normed, value_full, preferred_element_type=jnp.float32)
    gating = jnp.dot(normed, gate_full, preferred_element_type=jnp.float32)
    glu_out = values * jax.nn.sigmoid(gating)
    mixed_pos = causal_conv(glu_out, mix_taps.astype(jnp.float32))
    head_out = jax.nn.silu(head_norm(mixed_pos, head_gain)).astype(jnp.bfloat16)
    out_cols = out_full.shape[1]
    mixer_sum = jnp.dot(
        lax.all_gather(head_out, "tp", axis=1, tiled=True),
        out_full,
        preferred_element_type=jnp.float32,
    )
    own_cols = lax.dynamic_slice_in_dim(sequence, lax.axis_index("tp") * out_cols, out_cols, 1)
    hidden_cols = (own_cols.astype(jnp.float32) + mixer_sum).astype(jnp.bfloat16)
    full_rows = lax.all_gather(hidden_cols, "tp", axis=1, tiled=True)
    normed_ffn = row_norm(full_rows, ffn_gain)
    block_rows = normed_ffn
    ffgate = jnp.dot(
        block_rows,
        lax.all_gather(ffgate_weight, "fs", axis=0, tiled=True),
        preferred_element_type=jnp.float32,
    )
    ff_up = jnp.dot(
        block_rows,
        lax.all_gather(up_weight, "fs", axis=0, tiled=True),
        preferred_element_type=jnp.float32,
    )
    down_full = lax.all_gather(down_weight, "fs", axis=0, tiled=True)
    product = (jax.nn.silu(causal_conv(ffgate, ff_taps.astype(jnp.float32))) * ff_up).astype(
        jnp.bfloat16
    )
    own_count = sequence.shape[0] // lax.axis_size("tp")
    block_rows = product
    summed_rows = lax.psum_scatter(
        lax.dot_general(
            block_rows, down_full, (((1,), (1,)), ((), ())), preferred_element_type=jnp.float32
        ).astype(jnp.bfloat16),
        "tp",
        scatter_dimension=0,
        tiled=True,
    ).astype(jnp.float32)
    own_rows = lax.dynamic_slice_in_dim(full_rows, lax.axis_index("tp") * own_count, own_count, 0)
    return (own_rows.astype(jnp.float32) + summed_rows).astype(jnp.bfloat16)[None]


def solution(mesh):
    placed = (
        P(("rep", "fs"), None, None),
        P(),
        P("fs", "tp"),
        P("fs", "tp"),
        P(None, "tp"),
        P("tp"),
        P("fs", "tp"),
        P(),
        P("fs", "tp"),
        P("fs", "tp"),
        P(None, "tp"),
        P("fs", "tp"),
    )
    return jax.shard_map(
        on_device,
        mesh=mesh,
        in_specs=placed,
        out_specs=P(("rep", "fs"), "tp", None),
        check_vma=False,
    )
```

profile of v0, /device:TPU:0, one launch (start us, length us, event | category | flops | bytes accessed | tf_op | source)
XLA Modules:
  0.0 585.6 jit_solution(9061015034751386322)
XLA Ops:
  6.5 0.7 all-gather.11.cloned.1.call-update
  7.3 0.7 all-gather.9.cloned.1.call-update
  8.1 0.7 all-gather.15.cloned.1.call-update
  8.8 1.0 fusion.38
  9.8 1.0 fusion.39
  10.8 3.1 fusion.3
  13.9 0.7 convert_element_type.65
  14.6 0.7 convert_element_type.68
  15.2 24.4 %all-gather.11.cloned.1.call-done = bf16[2048,256]{1,0:T(8,128)(2,1)} async-done(((bf16[512,256]{1,0:T(8,128)(2,1)}), bf16[2048,256]{1,0:T(8,128)(2,1)}) %all-gather.11.cloned.1.call-update) | async-done | bytes 1048592 | tf_op jit(solution)/shard_map/all_gather | solution.py:54
  39.6 3.8 fusion.9
  43.5 25.1 %all-gather.9.cloned.1.call-done = bf16[2048,256]{1,0:T(8,128)(2,1)} async-done(((bf16[512,256]{1,0:T(8,128)(2,1)}), bf16[2048,256]{1,0:T(8,128)(2,1)}) %all-gather.9.cloned.1.call-update) | async-done | bytes 1048592 | tf_op jit(solution)/shard_map/all_gather | solution.py:53
  68.6 3.8 convolution_multiply_fusion
  72.4 4.2 multiply_add_fusion
  76.6 0.5 reshape.42
  77.2 1.1 reduce_sum.37
  78.4 14.4 %multiply_reduce_fusion = f32[1024,2]{1,0:T(8,128)S(1)} fusion(f32[1024,2,128]{2,1,0:T(2,128)S(1)} %reshape.42, f32[1024,2]{1,0:T(8,128)S(1)} %broadcast_multiply_fusion), kind=kLoop, calls=%fused_computation.26 | loop fusion | flops 784384 | bytes 1064960 | tf_op jit(solution)/shard_map/reduce_sum | solution.py:32
  92.9 1.2 mul.521
  94.1 1.2 sub.13
  95.4 5.8 multiply_convert_fusion.1
  101.3 22.2 %all-gather.13.cloned.1.call-done = bf16[1024,1024]{1,0:T(8,128)(2,1)} async-done(((bf16[1024,256]{1,0:T(8,128)(2,1)}), bf16[1024,1024]{1,0:T(8,128)(2,1)}) %all-gather.13.cloned.1.call-update) | async-done | bytes 2097168 | tf_op jit(solution)/shard_map/all_gather | solution.py:65
  123.5 4.4 fusion.6
  128.6 0.7 all-gather.21.cloned.1.call-update
  129.3 0.7 all-gather.23.cloned.1.call-update
  130.2 32.4 %all-gather.17.cloned.1.call-done = bf16[1024,2048]{1,0:T(8,128)(2,1)} async-done(((bf16[1024,512]{1,0:T(8,128)(2,1)}), bf16[1024,2048]{1,0:T(8,128)(2,1)}) %all-gather.17.cloned.1.call-update) | async-done | bytes 4194320 | tf_op jit(solution)/shard_map/all_gather | solution.py:71
  162.6 3.1 fusion
  165.7 113.7 %all-gather.19.cloned.1.call-done = bf16[2048,1536]{1,0:T(8,128)(2,1)} async-done(((bf16[512,1536]{1,0:T(8,128)(2,1)}), bf16[2048,1536]{1,0:T(8,128)(2,1)}) %all-gather.19.cloned.1.call-update) | async-done | bytes 6291472 | tf_op jit(solution)/shard_map/all_gather | solution.py:76
  279.4 12.2 %fusion.11 = f32[1024,1536]{1,0:T(8,128)} fusion(bf16[2048,1536]{1,0:T(8,128)(2,1)} %all-gather.19.cloned.1.call-done, bf16[1024,2048]{1,0:T(8,128)(2,1)} %all-gather.17.cloned.1.call-done, f32[2048]{0:T(1024)S(1)} %convert_element_type.73, f32[1024]{0:T(1024)S(1)} %add_rsqrt_fusion.1), kind=kOutput, calls=%fused_computation.20 | convolution fusion | flops 6450839552 | bytes 16789504 | tf_op jit(solution)/shard_map/dot_general | solution.py:74
  291.5 102.9 %all-gather.21.cloned.1.call-done = bf16[2048,1536]{1,0:T(8,128)(2,1)} async-done(((bf16[512,1536]{1,0:T(8,128)(2,1)}), bf16[2048,1536]{1,0:T(8,128)(2,1)}) %all-gather.21.cloned.1.call-update) | async-done | bytes 6291472 | tf_op jit(solution)/shard_map/all_gather | solution.py:81
  394.5 115.1 %all-gather.23.cloned.1.call-done = bf16[2048,1536]{1,0:T(8,128)(2,1)} async-done(((bf16[512,1536]{1,0:T(8,128)(2,1)}), bf16[2048,1536]{1,0:T(8,128)(2,1)}) %all-gather.23.cloned.1.call-update) | async-done | bytes 6291472 | tf_op jit(solution)/shard_map/all_gather | solution.py:84
  509.6 23.6 %convolution_convert_fusion = bf16[1024,2048]{1,0:T(8,128)(2,1)} fusion(bf16[2048,1536]{1,0:T(8,128)(2,1)} %all-gather.23.cloned.1.call-done, f32[1024,1536]{1,0:T(8,128)} %fusion.11, bf16[2048,1536]{1,0:T(8,128)(2,1)} %all-gather.21.cloned.1.call-done, f32[1536]{0:T(1024)S(1)} %get-tuple-element.6, f32[1536]{0:T(1024)S(1)} %get-tuple-element.7, ...), kind=kOutput, calls=%fused_computation.11 | convolution fusion | flops 12912689152 | bytes 27293696 | tf_op jit(solution)/shard_map/dot_general | solution.py:91
  533.2 42.9 %reduce-scatter.2.cloned.1.call-done = bf16[256,2048]{1,0:T(8,128)(2,1)} async-done(((bf16[1024,2048]{1,0:T(8,128)(2,1)}), bf16[256,2048]{1,0:T(8,128)(2,1)}) %reduce-scatter.2.cloned.1.call-update) | async-done | bytes 1048592 | tf_op jit(solution)/shard_map/reduce_scatter | solution.py:90
  576.1 2.9 fusion.15
  (25 shorter events, 1.1 us)
Async XLA Ops:
  6.5 33.1 %all-gather.11.cloned.1.call-start = ((), (), s32[]{:S(2)}) async-start(), calls=%async_computation.2 | async-start | bytes 1310720 | tf_op jit(solution)/shard_map/all_gather | solution.py:54
  7.3 61.3 %all-gather.9.cloned.1.call-start = ((), (), s32[]{:S(2)}) async-start(), calls=%async_computation.1 | async-start | bytes 1310720 | tf_op jit(solution)/shard_map/all_gather | solution.py:53
  8.0 93.3 %all-gather.15.cloned.1.call-start = ((), (), s32[]{:S(2)}) async-start(), calls=%async_computation.4 | async-start | bytes 1310720 | tf_op jit(solution)/shard_map/all_gather | solution.py:55
  8.7 114.8 %all-gather.13.cloned.1.call-start = ((), (), s32[]{:S(2)}) async-start(), calls=%async_computation.3 | async-start | bytes 2621440 | tf_op jit(solution)/shard_map/all_gather | solution.py:65
  101.2 61.4 %all-gather.17.cloned.1.call-start = ((), (), s32[]{:S(2)}) async-start(), calls=%async_computation.5 | async-start | bytes 5242880 | tf_op jit(solution)/shard_map/all_gather | solution.py:71
  101.2 28.8 %copy-start.1 = (bf16[2048]{0:T(1024)(128)(2,1)S(1)}, bf16[2048]{0:T(1024)(128)(2,1)}, u32[]{:S(2)}) copy-start(bf16[2048]{0:T(1024)(128)(2,1)} %param.19) | copy-start | bytes 12292
  101.3 28.9 %copy-start = (bf16[3,1536]{1,0:T(4,128)(2,1)S(1)}, bf16[3,1536]{1,0:T(4,128)(2,1)}, u32[]{:S(2)}) copy-start(bf16[3,1536]{1,0:T(4,128)(2,1)} %param.22) | copy-start | bytes 27652
  128.0 151.4 %all-gather.19.cloned.1.call-start = ((), (), s32[]{:S(2)}) async-start(), calls=%async_computation.6 | async-start | bytes 7864320 | tf_op jit(solution)/shard_map/all_gather | solution.py:76
  128.5 265.9 %all-gather.21.cloned.1.call-start = ((), (), s32[]{:S(2)}) async-start(), calls=%async_computation.7 | async-start | bytes 7864320 | tf_op jit(solution)/shard_map/all_gather | solution.py:81
  129.3 380.3 %all-gather.23.cloned.1.call-start = ((), (), s32[]{:S(2)}) async-start(), calls=%async_computation.8 | async-start | bytes 7864320 | tf_op jit(solution)/shard_map/all_gather | solution.py:84
  130.0 446.1 %reduce-scatter.2.cloned.1.call-start = ((), (), s32[]{:S(2)}) async-start(), calls=%async_computation.9 | async-start | bytes 5242880 | tf_op jit(solution)/shard_map/reduce_scatter | solution.py:90
Sparse Core Ops, SparseCore 0:
  8.9 30.6 all-gather.10
  41.2 27.3 all-gather.8
  70.2 27.3 all-gather.14
  101.3 22.1 all-gather.12
  128.1 34.4 all-gather.16
  164.0 115.3 all-gather.18
  280.9 113.4 all-gather.20
  396.0 113.5 all-gather.22
  533.3 42.7 reduce-scatter.1
where the time goes:
time: 586 us
  waiting for transfers between devices  483 us (82%)
  matrix products  47.8 us (8%)
  other arithmetic  36.1 us (6%)
  between operations  13.4 us (2%)
    all_gather x1, waiting for transfers between devices, on_device(): down_full = lax.all_gather(down_weight, 'fs', axis=0, tiled=True)  115 us
    all_gather x1, waiting for transfers between devices, on_device(): lax.all_gather(ffgate_weight, 'fs', axis=0, tiled=True)  114 us
    all_gather x1, waiting for transfers between devices, on_device(): lax.all_gather(up_weight, 'fs', axis=0, tiled=True)  103 us
    reduce_scatter x1, waiting for transfers between devices, on_device(): lax.psum_scatter(lax.dot_general(block_rows, down_full, (((1,), (1,)), ((...  42.9 us
    all_gather x1, waiting for transfers between devices, on_device(): full_rows = lax.all_gather(hidden_cols, 'tp', axis=1, tiled=True)  32.4 us
    all_gather x1, waiting for transfers between devices, on_device(): lax.all_gather(value_weight, 'fs', axis=0, tiled=True)  25.1 us
    all_gather x1, waiting for transfers between devices, on_device(): lax.all_gather(gate_weight, 'fs', axis=0, tiled=True)  24.4 us
    dot_general x1, matrix products, on_device(): lax.dot_general(block_rows, down_full, (((1,), (1,)), ((), ())), preferre...  23.6 us
  transfers between devices with their start and end apart: 9, of which 8 were waited for; matrix products, arithmetic and copies ran while one was open for 10% of the time, Pallas kernels for 0%

commit v1 on v0

v1 whole, which is shorter than its diff:
```python
import jax
import jax.numpy as jnp
from jax import lax
from jax.sharding import PartitionSpec as P


HEAD = 128


norm_floor = 0.01


def row_norm(floats_in, scales):
    floats = floats_in.astype(jnp.float32)
    scaled = floats * lax.rsqrt(jnp.mean(floats * floats, axis=-1, keepdims=True) + norm_floor)
    return (scaled * scales.astype(jnp.float32)).astype(jnp.bfloat16)


def causal_conv(signal, kernel_taps):
    reach = kernel_taps.shape[0]
    length = signal.shape[0]
    padded = jnp.pad(signal, ((reach - 1, 0), (0, 0)))
    summed = padded[0:length] * kernel_taps[0]
    for offset in range(1, reach):
        summed = summed + padded[offset : offset + length] * kernel_taps[offset]
    return summed


def head_norm(signal, scales):
    heads = []
    for start in range(0, signal.shape[1], HEAD):
        part = signal[:, start : start + HEAD]
        centre = part - jnp.mean(part, axis=-1, keepdims=True)
        spread = jnp.mean(centre * centre, axis=-1, keepdims=True)
        gain = scales[start : start + HEAD].astype(jnp.float32)
        heads.append(jax.nn.silu(centre * lax.rsqrt(spread + norm_floor) * gain))
    return jnp.concatenate(heads, axis=1).astype(jnp.bfloat16)


def fits(rows):
    return lax.axis_size("fs") == 4 and lax.axis_size("rep") == 2 and rows % 32 == 0


def pieces_of(shard):
    n = lax.axis_size("fs")
    f, r = lax.axis_index("fs"), lax.axis_index("rep")
    half = shard.shape[0] // 2
    mine = lax.dynamic_slice_in_dim(shard, r * half, half, 0)
    far = lax.ppermute(mine, "fs", [(0, 2), (1, 3), (2, 0), (3, 1)])
    up = lax.ppermute(mine, "fs", [(0, 1), (1, 2), (2, 3)])
    down = lax.ppermute(mine, "fs", [(1, 0), (2, 1), (3, 2)])
    last = lax.ppermute(far, "fs", [(2, 3), (1, 0)])

    def swap(block, members):
        pairs = []
        for m in members:
            pairs += [(m, n + m), (n + m, m)]
        return lax.ppermute(block, ("rep", "fs"), pairs)

    far_x = swap(far, (0, 1, 2, 3))
    up_x, down_x = swap(up, (1, 2, 3)), swap(down, (0, 1, 2))
    last_x = swap(last, (0, 3))
    low, high = f == 0, f == n - 1
    before, before_x = jnp.where(low, last, up), jnp.where(low, last_x, up_x)
    after, after_x = jnp.where(high, last, down), jnp.where(high, last_x, down_x)
    o = 1 - r
    return [
        ((f + 2) % n, r, far),
        ((f + 2) % n, o, far_x),
        ((f + n - 1) % n, r, before),
        ((f + 1) % n, r, after),
        ((f + n - 1) % n, o, before_x),
        ((f + 1) % n, o, after_x),
    ]


def gather_rows(shard):
    if not fits(shard.shape[0]):
        return lax.all_gather(shard, "fs", axis=0, tiled=True)
    n = lax.axis_size("fs")
    rows = shard.shape[0]
    full = jnp.zeros((n * rows, shard.shape[1]), shard.dtype)
    full = lax.dynamic_update_slice_in_dim(full, shard, lax.axis_index("fs") * rows, 0)
    for s, h, block in pieces_of(shard):
        full = lax.dynamic_update_slice_in_dim(full, block, s * rows + h * (rows // 2), 0)
    return full


def gather_small(shard):
    if not fits(shard.shape[0]):
        return lax.all_gather(shard, "fs", axis=0, tiled=True)
    n = lax.axis_size("fs")
    f, r = lax.axis_index("fs"), lax.axis_index("rep")
    rows = shard.shape[0]
    half = rows // 2
    mine = lax.dynamic_slice_in_dim(shard, r * half, half, 0)
    full = jnp.zeros((n * rows, shard.shape[1]), shard.dtype)
    full = lax.dynamic_update_slice_in_dim(full, shard, f * rows, 0)
    swaps = [(m, (m + n) % (2 * n)) for m in range(2 * n)]
    for hop in range(1, n):
        pairs = [(m, (m + hop) % n) for m in range(n)]
        here = lax.ppermute(mine, "fs", pairs)
        there = lax.ppermute(here, ("rep", "fs"), swaps)
        base = (f + n - hop) % n * rows
        full = lax.dynamic_update_slice_in_dim(full, here, base + r * half, 0)
        full = lax.dynamic_update_slice_in_dim(full, there, base + (1 - r) * half, 0)
    return full


def tp_scatter(block):
    size = lax.axis_size("tp")
    if size != 4:
        return lax.psum_scatter(block, "tp", scatter_dimension=0, tiled=True)
    t = lax.axis_index("tp")
    y, c = t // 2, t % 2
    parts = block.reshape(2, 2, block.shape[0] // size, block.shape[1])
    theirs = lax.dynamic_index_in_dim(parts, 1 - c, 1, keepdims=False)
    mine = lax.dynamic_index_in_dim(parts, c, 1, keepdims=False)
    got = lax.ppermute(theirs, "tp", [(0, 1), (1, 0), (2, 3), (3, 2)])

    def row_of(i):
        a = lax.dynamic_index_in_dim(mine, i, 0, keepdims=False).astype(jnp.float32)
        return a + lax.dynamic_index_in_dim(got, i, 0, keepdims=False).astype(jnp.float32)

    away = row_of(1 - y).astype(jnp.bfloat16)
    other = lax.ppermute(away, "tp", [(0, 2), (2, 0), (1, 3), (3, 1)])
    return row_of(y) + other.astype(jnp.float32)


def down_sums(product, shard, spread):
    n = lax.axis_size("fs")
    f, r = lax.axis_index("fs"), lax.axis_index("rep")
    rows = shard.shape[0]
    half = rows // 2

    def partial(weights):
        return lax.dot_general(
            product, weights, (((1,), (1,)), ((), ())), preferred_element_type=jnp.float32
        ).astype(jnp.bfloat16)

    early = partial(jnp.concatenate([shard] + [block for _, _, block in spread[:2]], axis=0))
    late = partial(jnp.concatenate([block for _, _, block in spread[2:]], axis=0))
    early, late = tp_scatter(early), tp_scatter(late)
    own = early[:, :rows]
    parts = [late[:, i * half : (i + 1) * half] for i in range(4)]

    def in_order(a, b):
        return jnp.concatenate([jnp.where(r == 0, a, b), jnp.where(r == 0, b, a)], axis=1)

    far = in_order(early[:, rows : rows + half], early[:, rows + half : 2 * rows])
    blocks = [own, in_order(parts[1], parts[3]), far, in_order(parts[0], parts[2])]
    return jnp.concatenate(
        [lax.select_n((s + n - f) % n, *blocks) for s in range(n)], axis=1
    )


def on_device(
    tokens,
    mix_gain,
    value_weight,
    gate_weight,
    mix_taps,
    head_gain,
    out_weight,
    ffn_gain,
    ffgate_weight,
    up_weight,
    ff_taps,
    down_weight,
):
    sequence = tokens[0]
    width = value_weight.shape[1]
    pair_full = gather_small(jnp.concatenate([value_weight, gate_weight], axis=1))
    out_full = lax.all_gather(out_weight, "fs", axis=0, tiled=True)
    normed = row_norm(sequence, mix_gain)
    both = jnp.dot(normed, pair_full, preferred_element_type=jnp.float32)
    glu_out = both[:, :width] * jax.nn.sigmoid(both[:, width:])
    mixed_pos = causal_conv(glu_out, mix_taps.astype(jnp.float32))
    head_out = head_norm(mixed_pos, head_gain)
    out_cols = out_full.shape[1]
    all_heads = lax.all_gather(head_out, "tp", axis=1, tiled=True)
    own_cols = lax.dynamic_slice_in_dim(sequence, lax.axis_index("tp") * out_cols, out_cols, 1)
    mixer_sum = jnp.dot(all_heads, out_full, preferred_element_type=jnp.float32)
    hidden_cols = (own_cols.astype(jnp.float32) + mixer_sum).astype(jnp.bfloat16)
    full_rows = lax.all_gather(hidden_cols, "tp", axis=1, tiled=True)
    normed_ffn = row_norm(full_rows, ffn_gain)
    gate_all = gather_rows(ffgate_weight)
    up_all = gather_rows(up_weight)
    ffgate = jnp.dot(normed_ffn, gate_all, preferred_element_type=jnp.float32)
    gated = jax.nn.silu(causal_conv(ffgate, ff_taps.astype(jnp.float32)))
    ff_up = jnp.dot(normed_ffn, up_all, preferred_element_type=jnp.float32)
    product = lax.optimization_barrier((gated * ff_up).astype(jnp.bfloat16))
    own_count = sequence.shape[0] // lax.axis_size("tp")
    own_rows = lax.dynamic_slice_in_dim(full_rows, lax.axis_index("tp") * own_count, own_count, 0)
    if fits(down_weight.shape[0]):
        spread = pieces_of(down_weight)
        result = down_sums(product, down_weight, spread)
    else:
        down_full = lax.all_gather(down_weight, "fs", axis=0, tiled=True)
        partial = lax.dot_general(
            product, down_full, (((1,), (1,)), ((), ())), preferred_element_type=jnp.float32
        )
        result = lax.psum_scatter(
            partial.astype(jnp.bfloat16), "tp", scatter_dimension=0, tiled=True
        )
    return (own_rows.astype(jnp.float32) + result.astype(jnp.float32)).astype(jnp.bfloat16)[None]


def solution(mesh):
    placed = (
        P(("rep", "fs"), None, None),
        P(),
        P("fs", "tp"),
        P("fs", "tp"),
        P(None, "tp"),
        P("tp"),
        P("fs", "tp"),
        P(),
        P("fs", "tp"),
        P("fs", "tp"),
        P(None, "tp"),
        P("fs", "tp"),
    )

    return jax.shard_map(
        on_device,
        mesh=mesh,
        in_specs=placed,
        out_specs=P(("rep", "fs"), "tp", None),
        check_vma=False,
    )
```

time: 586 us -> 435 us (0.74)
  waiting for transfers between devices: 483 us -> 230 us
  starting transfers between devices: 0.31 us -> 89.5 us
  local copies, waits for them, and re-layouts: 5.05 us -> 24 us
    all_gather x7 -> x2, waiting for transfers between devices: 404 us -> 0.04 us  [the longest x1 0.02 us: on_device(): out_full = lax.all_gather(out_weight, 'fs', axis=0, tiled=True)]
    ppermute x0 -> x34, waiting for transfers between devices: none -> 230 us  [the longest x12 80.9 us: swap(): return lax.ppermute(block, ('rep', 'fs'), pairs)]
    ppermute x0 -> x34, starting transfers between devices: none -> 89.5 us  [the longest x3 35.6 us: pieces_of(): up = lax.ppermute(mine, 'fs', [(0, 1), (1, 2), (2, 3)])]
    reduce_scatter x1 -> x0, waiting for transfers between devices: 42.9 us -> none  [on_device(): lax.psum_scatter(lax.dot_general(block_rows, down_full, (((1,), (1,)), ((...]
    all_gather x1, waiting for transfers between devices: 32.4 us -> 0.02 us  [on_device(): full_rows = lax.all_gather(hidden_cols, 'tp', axis=1, tiled=True)]
    reduce_sum x1, other arithmetic: 14.4 us -> 0.63 us  [head_norm(): spread = jnp.mean(centre * centre, axis=-1, keepdims=True)]
    dynamic_update_slice x0 -> x13, local copies, waits for them, and re-layouts: none -> 10.2 us  [the longest x4 7.35 us: gather_rows(): lax.dynamic_update_slice_in_dim(full, block, s * rows + h * (rows // 2), 0)]
    dynamic_update_slice x0 -> x8, other arithmetic: none -> 9.77 us  [gather_rows(): lax.dynamic_update_slice_in_dim(full, block, s * rows + h * (rows // 2), 0)]
  transfers between devices with their start and end apart: 9 -> 37, of which waited for: 8 -> 17; matrix products, arithmetic and copies ran while one was open for 10% -> 22% of each run, Pallas kernels for 0% -> 0%
where the time goes in v1:
time: 435 us; the launch traced here: 434 us
  waiting for transfers between devices  230 us (53%)
  starting transfers between devices  89.5 us (21%)
  matrix products  43.5 us (10%)
  other arithmetic  32.9 us (8%)
  local copies, waits for them, and re-layouts  24 us (6%)
  between operations  13.8 us (3%)
    ppermute x12, waiting for transfers between devices, swap(): return lax.ppermute(block, ('rep', 'fs'), pairs)  80.9 us
    ppermute x3, waiting for transfers between devices, pieces_of(): far = lax.ppermute(mine, 'fs', [(0, 2), (1, 3), (2, 0), (3, 1)])  56.3 us
    ppermute x3, starting transfers between devices, pieces_of(): up = lax.ppermute(mine, 'fs', [(0, 1), (1, 2), (2, 3)])  35.6 us
    ppermute x3, waiting for transfers between devices, pieces_of(): last = lax.ppermute(far, 'fs', [(2, 3), (1, 0)])  29.5 us
    ppermute x12, starting transfers between devices, swap(): return lax.ppermute(block, ('rep', 'fs'), pairs)  26 us
    ppermute x3, waiting for transfers between devices, gather_small(): here = lax.ppermute(mine, 'fs', pairs)  21 us
    ppermute x2, waiting for transfers between devices, tp_scatter(): other = lax.ppermute(away, 'tp', [(0, 2), (2, 0), (1, 3), (3, 1)])  20.3 us
    dot_general x1, matrix products, on_device(): ff_up = jnp.dot(normed_ffn, up_all, preferred_element_type=jnp.float32)  15.7 us
  transfers between devices with their start and end apart: 37, of which 17 were waited for; matrix products, arithmetic and copies ran while one was open for 22% of the time, Pallas kernels for 0%

profile of v1, /device:TPU:0, one launch (start us, length us, event | category | flops | bytes accessed | tf_op | source)
XLA Modules:
  0.0 434.0 jit_solution(14371438310391667676)
XLA Ops:
  23.0 18.8 %collective-permute-done.2 = bf16[256,512]{1,0:T(8,128)(2,1)S(1)} collective-permute-done((bf16[256,512]{1,0:T(8,128)(2,1)S(1)}, bf16[256,512]{1,0:T(8,128)(2,1)S(1)}, u32[]{:S(2)}, u32[]{:S(2)}) %collective-permute-start.2) | collective-permute-done | bytes 262176 | tf_op jit(solution)/shard_map/ppermute | solution.py:102
  43.9 7.0 %collective-permute-done.3 = bf16[256,512]{1,0:T(8,128)(2,1)S(1)} collective-permute-done((bf16[256,512]{1,0:T(8,128)(2,1)S(1)}, bf16[256,512]{1,0:T(8,128)(2,1)S(1)}, u32[]{:S(2)}, u32[]{:S(2)}) %collective-permute-start.3) | collective-permute-done | bytes 262176 | tf_op jit(solution)/shard_map/ppermute | solution.py:103
  51.0 4.4 %collective-permute-done.5 = bf16[256,512]{1,0:T(8,128)(2,1)S(1)} collective-permute-done((bf16[256,512]{1,0:T(8,128)(2,1)S(1)}, bf16[256,512]{1,0:T(8,128)(2,1)S(1)}, u32[]{:S(2)}, u32[]{:S(2)}) %collective-permute-start.5) | collective-permute-done | bytes 262176 | tf_op jit(solution)/shard_map/ppermute | solution.py:103
  58.2 4.0 multiply_add_fusion
  66.0 5.3 %collective-permute-start.6 = (bf16[256,1536]{1,0:T(8,128)(2,1)}, bf16[256,1536]{1,0:T(8,128)(2,1)}, u32[]{:S(2)}, u32[]{:S(2)}) collective-permute-start(bf16[256,1536]{1,0:T(8,128)(2,1)} %constant_dynamic-slice_fusion.2), channel_id=1, source_target_pairs={{0,8},{4,12},{8,0},{12,4},{1,9},{5,13},{9,1},{13,5},{2,10},{6,14},... | collective-permute-start | bytes 2359304 | tf_op jit(solution)/shard_map/ppermute | solution.py:49
  71.3 6.9 %collective-permute-start.9 = (bf16[256,1536]{1,0:T(8,128)(2,1)}, bf16[256,1536]{1,0:T(8,128)(2,1)}, u32[]{:S(2)}, u32[]{:S(2)}) collective-permute-start(bf16[256,1536]{1,0:T(8,128)(2,1)} %constant_dynamic-slice_fusion.2), channel_id=1, source_target_pairs={{0,4},{4,8},{8,12},{1,5},{5,9},{9,13},{2,6},{6,10},{10,14},{3,7},{... | collective-permute-start | bytes 2359304 | tf_op jit(solution)/shard_map/ppermute | solution.py:50
  81.7 5.1 %collective-permute-start.17 = (bf16[256,1536]{1,0:T(8,128)(2,1)}, bf16[256,1536]{1,0:T(8,128)(2,1)}, u32[]{:S(2)}, u32[]{:S(2)}) collective-permute-start(bf16[256,1536]{1,0:T(8,128)(2,1)} %constant_dynamic-slice_fusion.1), channel_id=1, source_target_pairs={{0,4},{4,8},{8,12},{1,5},{5,9},{9,13},{2,6},{6,10},{10,14},{3,7},{... | collective-permute-start | bytes 2359304 | tf_op jit(solution)/shard_map/ppermute | solution.py:50
  86.9 20.0 %collective-permute-done.6 = bf16[256,1536]{1,0:T(8,128)(2,1)} collective-permute-done((bf16[256,1536]{1,0:T(8,128)(2,1)}, bf16[256,1536]{1,0:T(8,128)(2,1)}, u32[]{:S(2)}, u32[]{:S(2)}) %collective-permute-start.6) | collective-permute-done | bytes 786464 | tf_op jit(solution)/shard_map/ppermute | solution.py:49
  110.5 3.1 broadcast.99.clone
  119.3 36.3 %collective-permute-done.14 = bf16[256,1536]{1,0:T(8,128)(2,1)} collective-permute-done((bf16[256,1536]{1,0:T(8,128)(2,1)}, bf16[256,1536]{1,0:T(8,128)(2,1)}, u32[]{:S(2)}, u32[]{:S(2)}) %collective-permute-start.14) | collective-permute-done | bytes 786464 | tf_op jit(solution)/shard_map/ppermute | solution.py:49
  157.0 4.4 %fusion.26 = bf16[1024,512]{1,0:T(8,128)(2,1)} fusion(bf16[1024,1024]{1,0:T(8,128)(2,1)} %all-gather.4.cloned.1.call-done, bf16[1024,512]{1,0:T(8,128)(2,1)} %all-gather.6.cloned.1.call-done, bf16[1,1024,2048]{2,1,0:T(8,128)(2,1)} %param.12, s32[]{:T(128)S(6)} %select_n.331), kind=kOutput, calls=%fused_computation.32 | convolution fusion | flops 1075314688 | bytes 5242884 | tf_op jit(solution)/shard_map/dot_general | solution.py:183
  169.1 23.5 %collective-permute-start.27 = (bf16[256,1536]{1,0:T(8,128)(2,1)}, bf16[256,1536]{1,0:T(8,128)(2,1)S(1)}, u32[]{:S(2)}, u32[]{:S(2)}) collective-permute-start(bf16[256,1536]{1,0:T(8,128)(2,1)} %constant_dynamic-slice_fusion), channel_id=1, source_target_pairs={{0,4},{4,8},{8,12},{1,5},{5,9},{9,13},{2,6},{6,10},{10,14},{3,7},{... | collective-permute-start | bytes 2359304 | tf_op jit(solution)/shard_map/ppermute | solution.py:50
  201.3 11.7 %collective-permute-done.15 = bf16[256,1536]{1,0:T(8,128)(2,1)S(1)} collective-permute-done((bf16[256,1536]{1,0:T(8,128)(2,1)}, bf16[256,1536]{1,0:T(8,128)(2,1)S(1)}, u32[]{:S(2)}, u32[]{:S(2)}) %collective-permute-start.15) | collective-permute-done | bytes 786464 | tf_op jit(solution)/shard_map/ppermute | solution.py:58
  216.0 3.4 collective-permute-start.13
  219.4 10.8 %collective-permute-done.28 = bf16[256,1536]{1,0:T(8,128)(2,1)S(1)} collective-permute-done((bf16[256,1536]{1,0:T(8,128)(2,1)}, bf16[256,1536]{1,0:T(8,128)(2,1)S(1)}, u32[]{:S(2)}, u32[]{:S(2)}) %collective-permute-start.28) | collective-permute-done | bytes 786464 | tf_op jit(solution)/shard_map/ppermute | solution.py:51
  230.9 16.1 %collective-permute-done.26 = bf16[256,1536]{1,0:T(8,128)(2,1)S(1)} collective-permute-done((bf16[256,1536]{1,0:T(8,128)(2,1)}, bf16[256,1536]{1,0:T(8,128)(2,1)S(1)}, u32[]{:S(2)}, u32[]{:S(2)}) %collective-permute-start.26) | collective-permute-done | bytes 786464 | tf_op jit(solution)/shard_map/ppermute | solution.py:52
  247.1 3.4 collective-permute-start.21
  250.6 12.3 %collective-permute-done.16 = bf16[256,1536]{1,0:T(8,128)(2,1)S(1)} collective-permute-done((bf16[256,1536]{1,0:T(8,128)(2,1)}, bf16[256,1536]{1,0:T(8,128)(2,1)S(1)}, u32[]{:S(2)}, u32[]{:S(2)}) %collective-permute-start.16) | collective-permute-done | bytes 786464 | tf_op jit(solution)/shard_map/ppermute | solution.py:52
  262.9 3.4 collective-permute-start.11
  269.2 14.1 %collective-permute-done.11 = bf16[256,1536]{1,0:T(8,128)(2,1)S(1)} collective-permute-done((bf16[256,1536]{1,0:T(8,128)(2,1)S(1)}, bf16[256,1536]{1,0:T(8,128)(2,1)S(1)}, u32[]{:S(2)}, u32[]{:S(2)}) %collective-permute-start.11) | collective-permute-done | bytes 786464 | tf_op jit(solution)/shard_map/ppermute | solution.py:58
  283.3 3.4 collective-permute-start.19
  292.8 12.8 %collective-permute-done.19 = bf16[256,1536]{1,0:T(8,128)(2,1)S(1)} collective-permute-done((bf16[256,1536]{1,0:T(8,128)(2,1)S(1)}, bf16[256,1536]{1,0:T(8,128)(2,1)S(1)}, u32[]{:S(2)}, u32[]{:S(2)}) %collective-permute-start.19) | collective-permute-done | bytes 786464 | tf_op jit(solution)/shard_map/ppermute | solution.py:58
  305.6 3.4 collective-permute-start.29
  311.2 11.3 %collective-permute-done.31 = bf16[256,1536]{1,0:T(8,128)(2,1)S(1)} collective-permute-done((bf16[256,1536]{1,0:T(8,128)(2,1)S(1)}, bf16[256,1536]{1,0:T(8,128)(2,1)S(1)}, u32[]{:S(2)}, u32[]{:S(2)}) %collective-permute-start.31) | collective-permute-done | bytes 786464 | tf_op jit(solution)/shard_map/ppermute | solution.py:58
  322.4 31.0 %collective-permute-done.29 = bf16[256,1536]{1,0:T(8,128)(2,1)S(1)} collective-permute-done((bf16[256,1536]{1,0:T(8,128)(2,1)S(1)}, bf16[256,1536]{1,0:T(8,128)(2,1)S(1)}, u32[]{:S(2)}, u32[]{:S(2)}) %collective-permute-start.29) | collective-permute-done | bytes 786464 | tf_op jit(solution)/shard_map/ppermute | solution.py:58
  353.6 3.2 fusion
  357.0 10.6 %fusion.34 = f32[1024,1536]{1,0:T(8,128)} fusion(bf16[2048,1536]{1,0:T(8,128)(2,1)} %select_dynamic-update-slice_fusion.4, bf16[1024,2048]{1,0:T(8,128)(2,1)S(1)} %copy-done, f32[2048]{0:T(1024)S(1)} %convert_element_type.134, f32[1024]{0:T(1024)S(1)} %add_rsqrt_fusion), kind=kOutput, calls=%fused_computation.35 | convolution fusion | flops 6450839552 | bytes 16789504 | tf_op jit(solution)/shard_map/dot_general | solution.py:189
  367.7 15.7 %multiply_convert_fusion = bf16[1024,1536]{1,0:T(8,128)(2,1)S(1)} fusion(f32[1024,1536]{1,0:T(8,128)} %fusion.34, bf16[2048,1536]{1,0:T(8,128)(2,1)} %select_dynamic-update-slice_fusion, f32[1536]{0:T(1024)S(1)} %get-tuple-element.10, f32[1536]{0:T(1024)S(1)} %get-tuple-element.11, f32[1536]{0:T(1024)S(1)} %get-tuple-element.9, ...), kind=kOutput, calls=%fused_computation.10 | convolution fusion | flops 6468141056 | bytes 19953664 | tf_op jit(solution)/shard_map/dot_general | solution.py:191
  383.3 5.5 %fusion.27 = bf16[1024,1024]{1,0:T(8,128)(2,1)S(1)} fusion(bf16[1024,1536]{1,0:T(8,128)(2,1)S(1)} %multiply_convert_fusion, bf16[256,1536]{1,0:T(8,128)(2,1)S(1)} %get-tuple-element.23, bf16[256,1536]{1,0:T(8,128)(2,1)S(1)} %get-tuple-element.22, bf16[256,1536]{1,0:T(8,128)(2,1)S(1)} %get-tuple-element.21, bf16[256,1536]{1,0:T(8,128)(2,1)S(1)} %get-tuple-element.20), kind=kOutput, calls=%fused_computation.33 | convolution fusion | flops 3234856960 | bytes 8388608 | tf_op jit(solution)/shard_map/dot_general | solution.py:137
  390.1 4.8 %fusion.30 = bf16[1024,1024]{1,0:T(8,128)(2,1)S(1)} fusion(bf16[1024,1536]{1,0:T(8,128)(2,1)S(1)} %multiply_convert_fusion, bf16[256,1536]{1,0:T(8,128)(2,1)} %collective-permute-done.23, bf16[256,1536]{1,0:T(8,128)(2,1)} %collective-permute-done.22, bf16[512,1536]{1,0:T(8,128)(2,1)S(1)} %copy-done.5), kind=kOutput, calls=%fused_computation.34 | convolution fusion | flops 3231711232 | bytes 8388608 | tf_op jit(solution)/shard_map/dot_general | solution.py:137
  401.1 11.8 %collective-permute-done.33 = bf16[256,1024]{1,0:T(8,128)(2,1)} collective-permute-done((bf16[256,1024]{1,0:T(8,128)(2,1)}, bf16[256,1024]{1,0:T(8,128)(2,1)}, u32[]{:S(2)}, u32[]{:S(2)}) %collective-permute-start.33) | collective-permute-done | bytes 524320 | tf_op jit(solution)/shard_map/ppermute | solution.py:126
  414.6 8.5 %collective-permute-done.25 = bf16[256,1024]{1,0:T(8,128)(2,1)S(1)} collective-permute-done((bf16[256,1024]{1,0:T(8,128)(2,1)S(1)}, bf16[256,1024]{1,0:T(8,128)(2,1)S(1)}, u32[]{:S(2)}, u32[]{:S(2)}) %collective-permute-start.25) | collective-permute-done | bytes 524320 | tf_op jit(solution)/shard_map/ppermute | solution.py:126
  (138 shorter events, 84.0 us)
Async XLA Ops:
  6.5 150.4 %all-gather.6.cloned.1.call-start = ((), (), s32[]{:S(2)}) async-start(), calls=%async_computation.1 | async-start | bytes 1310720 | tf_op jit(solution)/shard_map/all_gather | solution.py:174
  11.7 30.1 %collective-permute-start.2 = (bf16[256,512]{1,0:T(8,128)(2,1)S(1)}, bf16[256,512]{1,0:T(8,128)(2,1)S(1)}, u32[]{:S(2)}, u32[]{:S(2)}) collective-permute-start(bf16[256,512]{1,0:T(8,128)(2,1)S(1)} %constant_dynamic-slice_fusion.3), channel_id=1, source_target_pairs={{0,8},{4,12},{8,0},{12,4},{1,9},{5,13},{9,1},{13,5},{2,10},{6,14},... | collective-permute-start | bytes 786440 | tf_op jit(solution)/shard_map/ppermute | solution.py:102
  14.3 28.9 %collective-permute-start.4 = (bf16[256,512]{1,0:T(8,128)(2,1)S(1)}, bf16[256,512]{1,0:T(8,128)(2,1)S(1)}, u32[]{:S(2)}, u32[]{:S(2)}) collective-permute-start(bf16[256,512]{1,0:T(8,128)(2,1)S(1)} %constant_dynamic-slice_fusion.3), channel_id=1, source_target_pairs={{0,12},{4,0},{8,4},{12,8},{1,13},{5,1},{9,5},{13,9},{2,14},{6,2},{... | collective-permute-start | bytes 786440 | tf_op jit(solution)/shard_map/ppermute | solution.py:102
  15.6 141.3 %all-gather.4.cloned.1.call-start = ((), (), s32[]{:S(2)}) async-start(), calls=%async_computation | async-start | bytes 2621440 | tf_op jit(solution)/shard_map/all_gather | solution.py:181
  21.0 22.8 %collective-permute-start.1 = (bf16[256,512]{1,0:T(8,128)(2,1)S(1)}, bf16[256,512]{1,0:T(8,128)(2,1)S(1)}, u32[]{:S(2)}, u32[]{:S(2)}) collective-permute-start(bf16[256,512]{1,0:T(8,128)(2,1)S(1)} %collective-permute-done), channel_id=1, source_target_pairs={{0,16},{4,20},{8,24},{12,28},{16,0},{20,4},{24,8},{28,12},{1,17},{... | collective-permute-start | bytes 786440 | tf_op jit(solution)/shard_map/ppermute | solution.py:103
  65.0 288.6 %all-gather.8.cloned.1.call-start = ((), (), s32[]{:S(2)}) async-start(), calls=%async_computation.2 | async-start | bytes 5242880 | tf_op jit(solution)/shard_map/all_gather | solution.py:185
  66.0 40.9 %collective-permute-start.6 = (bf16[256,1536]{1,0:T(8,128)(2,1)}, bf16[256,1536]{1,0:T(8,128)(2,1)}, u32[]{:S(2)}, u32[]{:S(2)}) collective-permute-start(bf16[256,1536]{1,0:T(8,128)(2,1)} %constant_dynamic-slice_fusion.2), channel_id=1, source_target_pairs={{0,8},{4,12},{8,0},{12,4},{1,9},{5,13},{9,1},{13,5},{2,10},{6,14},... | collective-permute-start | bytes 2359304 | tf_op jit(solution)/shard_map/ppermute | solution.py:49
  71.3 96.5 %collective-permute-start.9 = (bf16[256,1536]{1,0:T(8,128)(2,1)}, bf16[256,1536]{1,0:T(8,128)(2,1)}, u32[]{:S(2)}, u32[]{:S(2)}) collective-permute-start(bf16[256,1536]{1,0:T(8,128)(2,1)} %constant_dynamic-slice_fusion.2), channel_id=1, source_target_pairs={{0,4},{4,8},{8,12},{1,5},{5,9},{9,13},{2,6},{6,10},{10,14},{3,7},{... | collective-permute-start | bytes 2359304 | tf_op jit(solution)/shard_map/ppermute | solution.py:50
  78.3 90.8 %collective-permute-start.10 = (bf16[256,1536]{1,0:T(8,128)(2,1)}, bf16[256,1536]{1,0:T(8,128)(2,1)}, u32[]{:S(2)}, u32[]{:S(2)}) collective-permute-start(bf16[256,1536]{1,0:T(8,128)(2,1)} %constant_dynamic-slice_fusion.2), channel_id=1, source_target_pairs={{4,0},{8,4},{12,8},{5,1},{9,5},{13,9},{6,2},{10,6},{14,10},{7,3},{... | collective-permute-start | bytes 2359304 | tf_op jit(solution)/shard_map/ppermute | solution.py:51
  80.5 75.1 %collective-permute-start.14 = (bf16[256,1536]{1,0:T(8,128)(2,1)}, bf16[256,1536]{1,0:T(8,128)(2,1)}, u32[]{:S(2)}, u32[]{:S(2)}) collective-permute-start(bf16[256,1536]{1,0:T(8,128)(2,1)} %constant_dynamic-slice_fusion.1), channel_id=1, source_target_pairs={{0,8},{4,12},{8,0},{12,4},{1,9},{5,13},{9,1},{13,5},{2,10},{6,14},... | collective-permute-start | bytes 2359304 | tf_op jit(solution)/shard_map/ppermute | solution.py:49
  81.7 110.9 %collective-permute-start.17 = (bf16[256,1536]{1,0:T(8,128)(2,1)}, bf16[256,1536]{1,0:T(8,128)(2,1)}, u32[]{:S(2)}, u32[]{:S(2)}) collective-permute-start(bf16[256,1536]{1,0:T(8,128)(2,1)} %constant_dynamic-slice_fusion.1), channel_id=1, source_target_pairs={{0,4},{4,8},{8,12},{1,5},{5,9},{9,13},{2,6},{6,10},{10,14},{3,7},{... | collective-permute-start | bytes 2359304 | tf_op jit(solution)/shard_map/ppermute | solution.py:50
  106.9 48.7 %collective-permute-start.7 = (bf16[256,1536]{1,0:T(8,128)(2,1)}, bf16[256,1536]{1,0:T(8,128)(2,1)}, u32[]{:S(2)}, u32[]{:S(2)}) collective-permute-start(bf16[256,1536]{1,0:T(8,128)(2,1)} %collective-permute-done.6), channel_id=1, source_target_pairs={{0,16},{16,0},{4,20},{20,4},{8,24},{24,8},{12,28},{28,12},{1,17},{... | collective-permute-start | bytes 2359304 | tf_op jit(solution)/shard_map/ppermute | solution.py:58
  155.6 38.3 %collective-permute-start.22 = (bf16[256,1536]{1,0:T(8,128)(2,1)}, bf16[256,1536]{1,0:T(8,128)(2,1)}, u32[]{:S(2)}, u32[]{:S(2)}) collective-permute-start(bf16[256,1536]{1,0:T(8,128)(2,1)} %constant_dynamic-slice_fusion), channel_id=1, source_target_pairs={{0,8},{4,12},{8,0},{12,4},{1,9},{5,13},{9,1},{13,5},{2,10},{6,14},... | collective-permute-start | bytes 2359304 | tf_op jit(solution)/shard_map/ppermute | solution.py:49
  155.6 40.9 %collective-permute-start.8 = (bf16[256,1536]{1,0:T(8,128)(2,1)}, bf16[256,1536]{1,0:T(8,128)(2,1)S(1)}, u32[]{:S(2)}, u32[]{:S(2)}) collective-permute-start(bf16[256,1536]{1,0:T(8,128)(2,1)} %collective-permute-done.6), channel_id=1, source_target_pairs={{8,12},{4,0},{9,13},{5,1},{10,14},{6,2},{11,15},{7,3},{24,28},{20,... | collective-permute-start | bytes 2359304 | tf_op jit(solution)/shard_map/ppermute | solution.py:52
  167.8 47.5 %collective-permute-start.18 = (bf16[256,1536]{1,0:T(8,128)(2,1)}, bf16[256,1536]{1,0:T(8,128)(2,1)S(1)}, u32[]{:S(2)}, u32[]{:S(2)}) collective-permute-start(bf16[256,1536]{1,0:T(8,128)(2,1)} %constant_dynamic-slice_fusion.1), channel_id=1, source_target_pairs={{4,0},{8,4},{12,8},{5,1},{9,5},{13,9},{6,2},{10,6},{14,10},{7,3},{... | collective-permute-start | bytes 2359304 | tf_op jit(solution)/shard_map/ppermute | solution.py:51
  169.1 46.9 %collective-permute-start.27 = (bf16[256,1536]{1,0:T(8,128)(2,1)}, bf16[256,1536]{1,0:T(8,128)(2,1)S(1)}, u32[]{:S(2)}, u32[]{:S(2)}) collective-permute-start(bf16[256,1536]{1,0:T(8,128)(2,1)} %constant_dynamic-slice_fusion), channel_id=1, source_target_pairs={{0,4},{4,8},{8,12},{1,5},{5,9},{9,13},{2,6},{6,10},{10,14},{3,7},{... | collective-permute-start | bytes 2359304 | tf_op jit(solution)/shard_map/ppermute | solution.py:50
  192.6 37.6 %collective-permute-start.28 = (bf16[256,1536]{1,0:T(8,128)(2,1)}, bf16[256,1536]{1,0:T(8,128)(2,1)S(1)}, u32[]{:S(2)}, u32[]{:S(2)}) collective-permute-start(bf16[256,1536]{1,0:T(8,128)(2,1)} %constant_dynamic-slice_fusion), channel_id=1, source_target_pairs={{4,0},{8,4},{12,8},{5,1},{9,5},{13,9},{6,2},{10,6},{14,10},{7,3},{... | collective-permute-start | bytes 2359304 | tf_op jit(solution)/shard_map/ppermute | solution.py:51
  193.9 19.1 %collective-permute-start.15 = (bf16[256,1536]{1,0:T(8,128)(2,1)}, bf16[256,1536]{1,0:T(8,128)(2,1)S(1)}, u32[]{:S(2)}, u32[]{:S(2)}) collective-permute-start(bf16[256,1536]{1,0:T(8,128)(2,1)} %collective-permute-done.14), channel_id=1, source_target_pairs={{0,16},{16,0},{4,20},{20,4},{8,24},{24,8},{12,28},{28,12},{1,17},{... | collective-permute-start | bytes 2359304 | tf_op jit(solution)/shard_map/ppermute | solution.py:58
  196.5 50.6 %collective-permute-start.26 = (bf16[256,1536]{1,0:T(8,128)(2,1)}, bf16[256,1536]{1,0:T(8,128)(2,1)S(1)}, u32[]{:S(2)}, u32[]{:S(2)}) collective-permute-start(bf16[256,1536]{1,0:T(8,128)(2,1)} %collective-permute-done.22), channel_id=1, source_target_pairs={{8,12},{4,0},{9,13},{5,1},{10,14},{6,2},{11,15},{7,3},{24,28},{20,... | collective-permute-start | bytes 2359304 | tf_op jit(solution)/shard_map/ppermute | solution.py:52
  213.0 49.9 %collective-permute-start.16 = (bf16[256,1536]{1,0:T(8,128)(2,1)}, bf16[256,1536]{1,0:T(8,128)(2,1)S(1)}, u32[]{:S(2)}, u32[]{:S(2)}) collective-permute-start(bf16[256,1536]{1,0:T(8,128)(2,1)} %collective-permute-done.14), channel_id=1, source_target_pairs={{8,12},{4,0},{9,13},{5,1},{10,14},{6,2},{11,15},{7,3},{24,28},{20,... | collective-permute-start | bytes 2359304 | tf_op jit(solution)/shard_map/ppermute | solution.py:52
  215.3 53.2 %collective-permute-start.12 = (bf16[256,1536]{1,0:T(8,128)(2,1)}, bf16[256,1536]{1,0:T(8,128)(2,1)S(1)}, u32[]{:S(2)}, u32[]{:S(2)}) collective-permute-start(bf16[256,1536]{1,0:T(8,128)(2,1)} %collective-permute-done.9), channel_id=1, source_target_pairs={{4,20},{20,4},{8,24},{24,8},{12,28},{28,12},{5,21},{21,5},{9,25},{... | collective-permute-start | bytes 2359304 | tf_op jit(solution)/shard_map/ppermute | solution.py:58
  216.0 71.8 %collective-permute-start.13 = (bf16[256,1536]{1,0:T(8,128)(2,1)}, bf16[256,1536]{1,0:T(8,128)(2,1)S(1)}, u32[]{:S(2)}, u32[]{:S(2)}) collective-permute-start(bf16[256,1536]{1,0:T(8,128)(2,1)} %collective-permute-done.10), channel_id=1, source_target_pairs={{0,16},{16,0},{4,20},{20,4},{8,24},{24,8},{1,17},{17,1},{5,21},{21... | collective-permute-start | bytes 2359304 | tf_op jit(solution)/shard_map/ppermute | solution.py:58
  230.2 61.0 %collective-permute-start.20 = (bf16[256,1536]{1,0:T(8,128)(2,1)}, bf16[256,1536]{1,0:T(8,128)(2,1)S(1)}, u32[]{:S(2)}, u32[]{:S(2)}) collective-permute-start(bf16[256,1536]{1,0:T(8,128)(2,1)} %collective-permute-done.17), channel_id=1, source_target_pairs={{4,20},{20,4},{8,24},{24,8},{12,28},{28,12},{5,21},{21,5},{9,25},{... | collective-permute-start | bytes 2359304 | tf_op jit(solution)/shard_map/ppermute | solution.py:58
  247.1 63.0 %collective-permute-start.21 = (bf16[256,1536]{1,0:T(8,128)(2,1)S(1)}, bf16[256,1536]{1,0:T(8,128)(2,1)S(1)}, u32[]{:S(2)}, u32[]{:S(2)}) collective-permute-start(bf16[256,1536]{1,0:T(8,128)(2,1)S(1)} %collective-permute-done.18), channel_id=1, source_target_pairs={{0,16},{16,0},{4,20},{20,4},{8,24},{24,8},{1,17},{17,1},{5,21},{21... | collective-permute-start | bytes 2359304 | tf_op jit(solution)/shard_map/ppermute | solution.py:58
  262.9 20.4 %collective-permute-start.11 = (bf16[256,1536]{1,0:T(8,128)(2,1)S(1)}, bf16[256,1536]{1,0:T(8,128)(2,1)S(1)}, u32[]{:S(2)}, u32[]{:S(2)}) collective-permute-start(bf16[256,1536]{1,0:T(8,128)(2,1)S(1)} %collective-permute-done.8), channel_id=1, source_target_pairs={{0,16},{16,0},{12,28},{28,12},{1,17},{17,1},{13,29},{29,13},{2,18}... | collective-permute-start | bytes 2359304 | tf_op jit(solution)/shard_map/ppermute | solution.py:58
  268.5 42.7 %collective-permute-start.30 = (bf16[256,1536]{1,0:T(8,128)(2,1)S(1)}, bf16[256,1536]{1,0:T(8,128)(2,1)S(1)}, u32[]{:S(2)}, u32[]{:S(2)}) collective-permute-start(bf16[256,1536]{1,0:T(8,128)(2,1)S(1)} %collective-permute-done.27), channel_id=1, source_target_pairs={{4,20},{20,4},{8,24},{24,8},{12,28},{28,12},{5,21},{21,5},{9,25},{... | collective-permute-start | bytes 2359304 | tf_op jit(solution)/shard_map/ppermute | solution.py:58
  283.3 22.3 %collective-permute-start.19 = (bf16[256,1536]{1,0:T(8,128)(2,1)S(1)}, bf16[256,1536]{1,0:T(8,128)(2,1)S(1)}, u32[]{:S(2)}, u32[]{:S(2)}) collective-permute-start(bf16[256,1536]{1,0:T(8,128)(2,1)S(1)} %collective-permute-done.16), channel_id=1, source_target_pairs={{0,16},{16,0},{12,28},{28,12},{1,17},{17,1},{13,29},{29,13},{2,18}... | collective-permute-start | bytes 2359304 | tf_op jit(solution)/shard_map/ppermute | solution.py:58
  287.8 34.6 %collective-permute-start.31 = (bf16[256,1536]{1,0:T(8,128)(2,1)S(1)}, bf16[256,1536]{1,0:T(8,128)(2,1)S(1)}, u32[]{:S(2)}, u32[]{:S(2)}) collective-permute-start(bf16[256,1536]{1,0:T(8,128)(2,1)S(1)} %collective-permute-done.28), channel_id=1, source_target_pairs={{0,16},{16,0},{4,20},{20,4},{8,24},{24,8},{1,17},{17,1},{5,21},{21... | collective-permute-start | bytes 2359304 | tf_op jit(solution)/shard_map/ppermute | solution.py:58
  291.3 98.8 %collective-permute-start.23 = (bf16[256,1536]{1,0:T(8,128)(2,1)}, bf16[256,1536]{1,0:T(8,128)(2,1)}, u32[]{:S(2)}, u32[]{:S(2)}) collective-permute-start(bf16[256,1536]{1,0:T(8,128)(2,1)} %collective-permute-done.22), channel_id=1, source_target_pairs={{0,16},{16,0},{4,20},{20,4},{8,24},{24,8},{12,28},{28,12},{1,17},{... | collective-permute-start | bytes 2359304 | tf_op jit(solution)/shard_map/ppermute | solution.py:58
  305.6 47.8 %collective-permute-start.29 = (bf16[256,1536]{1,0:T(8,128)(2,1)S(1)}, bf16[256,1536]{1,0:T(8,128)(2,1)S(1)}, u32[]{:S(2)}, u32[]{:S(2)}) collective-permute-start(bf16[256,1536]{1,0:T(8,128)(2,1)S(1)} %collective-permute-done.26), channel_id=1, source_target_pairs={{0,16},{16,0},{12,28},{28,12},{1,17},{17,1},{13,29},{29,13},{2,18}... | collective-permute-start | bytes 2359304 | tf_op jit(solution)/shard_map/ppermute | solution.py:58
  397.7 15.1 %collective-permute-start.33 = (bf16[256,1024]{1,0:T(8,128)(2,1)}, bf16[256,1024]{1,0:T(8,128)(2,1)}, u32[]{:S(2)}, u32[]{:S(2)}) collective-permute-start(bf16[256,1024]{1,0:T(8,128)(2,1)} %fusion.41), channel_id=1, source_target_pairs={{0,2},{2,0},{1,3},{3,1},{4,6},{6,4},{5,7},{7,5},{8,10},{10,8},{9,1... | collective-permute-start | bytes 1572872 | tf_op jit(solution)/shard_map/ppermute | solution.py:126
  400.5 22.5 %collective-permute-start.25 = (bf16[256,1024]{1,0:T(8,128)(2,1)S(1)}, bf16[256,1024]{1,0:T(8,128)(2,1)S(1)}, u32[]{:S(2)}, u32[]{:S(2)}) collective-permute-start(bf16[256,1024]{1,0:T(8,128)(2,1)S(1)} %fusion.43), channel_id=1, source_target_pairs={{0,2},{2,0},{1,3},{3,1},{4,6},{6,4},{5,7},{7,5},{8,10},{10,8},{9,1... | collective-permute-start | bytes 1572872 | tf_op jit(solution)/shard_map/ppermute | solution.py:126
  (16 other events, 214.7 us)
Sparse Core Ops, SparseCore 0:
  15.8 34.9 all-gather.5
  65.1 29.3 all-gather.3
  161.5 53.8 all-gather.7
